TPU v7x, 32 devices: a whole 2x2x4 slice. The times are simulated.
32 devices in a mesh: sp: 16 (over z, y, x), dp: 2 (over core).
Axes of the slice: x: 2, y: 2, z: 4, core: 2. Of those that a mesh axis runs over, the one named last changes fastest.
Arguments:
- val_input: bfloat16 [2048, 1536], P('sp', 'dp'), may hold values from -24 to 24, as said below
- gate_input: bfloat16 [2048, 1536], P('sp', 'dp'), may hold values from -8 to 8
- cotangent: bfloat16 [2048, 4096], P('sp'), may hold values from -6 to 6
- out_weight: bfloat16 [4096, 1536], P('sp', 'dp'), may hold values from -0.09375 to 0.09375
- conv_taps: float32 [31, 1536], P(None, 'dp'), may hold values from -1 to 1
- norm_gain: float32 [1536], P('dp'), may hold values from 0.1 to 1.9
Outputs:
- grad_val: bfloat16 [2048, 1536], P('sp', 'dp')
- grad_gate: bfloat16 [2048, 1536], P('sp', 'dp')
- grad_out_weight: float32 [4096, 1536], P('sp', 'dp')
- grad_taps: float32 [31, 1536], P(None, 'dp')
- grad_gain: float32 [1536], P('dp')
Inputs may be any that keep to these rules, and one draw needn't show every extreme that they name: `val_input`: blocks of 64 channels and blocks of 32 tokens carry their own scales.
All inputs are finite; a program needn't handle non-finite values.
Results may differ from a plain program's by a relative error of at most 0.0063.
Values may be sent and summed in bfloat16 or wider, within the bound.
A program may use at most 64 MiB of HBM per device.

v0:
```python
import jax
import jax.numpy as jnp
from jax import lax
from jax.sharding import PartitionSpec as P

norm_floor = 0.25


def body(val_input, gate_input, cotangent, out_weight, conv_taps, norm_gain):
    width_dp = val_input.shape[1]
    taps = conv_taps.shape[0]
    channels = width_dp * lax.axis_size("dp")
    columns = cotangent
    grad_mix = jnp.dot(
        columns,
        lax.all_gather(out_weight, "sp", axis=0, tiled=True),
        preferred_element_type=jnp.float32,
    )
    sigma_gate = jax.nn.sigmoid(gate_input.astype(jnp.float32))
    mixed_in = (val_input.astype(jnp.float32) * sigma_gate).astype(jnp.bfloat16)
    per_device = width_dp // lax.axis_size("sp")
    first_channel = lax.axis_index("sp") * per_device
    local_taps = lax.dynamic_slice_in_dim(conv_taps, first_channel, per_device, 1)
    by_channel = lax.all_to_all(mixed_in.T, "sp", split_axis=0, concat_axis=1, tiled=True)
    full_len = by_channel.shape[1]
    padded_in = jnp.pad(by_channel.astype(jnp.float32), ((0, 0), (taps - 1, 0)))
    conv_out = jnp.zeros((per_device, full_len), jnp.float32)
    for offset in range(taps):
        conv_out = conv_out + local_taps[offset][:, None] * padded_in[:, offset : offset + full_len]
    conv_back = lax.all_to_all(
        conv_out.astype(jnp.bfloat16), "sp", split_axis=1, concat_axis=0, tiled=True
    )
    conv_rows = conv_back.T.astype(jnp.float32)
    row_sums = lax.psum((jnp.sum(conv_rows, 1), jnp.sum(conv_rows * conv_rows, 1)), "dp")
    row_mean = row_sums[0][:, None] / channels
    row_var = row_sums[1][:, None] / channels - row_mean * row_mean
    inv_scale = lax.rsqrt(row_var + norm_floor)
    normed = (conv_rows - row_mean) * inv_scale
    act = normed * norm_gain[None, :]
    sigma_act = jax.nn.sigmoid(act)
    swished = (act * sigma_act).astype(jnp.bfloat16)
    columns = cotangent
    grad_out_weight = lax.psum_scatter(
        lax.dot_general(
            columns, swished, (((0,), (0,)), ((), ())), preferred_element_type=jnp.float32
        ),
        "sp",
        scatter_dimension=0,
        tiled=True,
    )
    grad_act = grad_mix * sigma_act * (1.0 + act * (1.0 - sigma_act))
    gain_part = jnp.sum(grad_act * normed, 0)
    grad_norm = grad_act * norm_gain[None, :]
    norm_sums = lax.psum((jnp.sum(grad_norm, 1), jnp.sum(grad_norm * normed, 1)), "dp")
    first_sum = norm_sums[0][:, None] / channels
    second_sum = norm_sums[1][:, None] / channels
    grad_conv = (inv_scale * (grad_norm - first_sum - normed * second_sum)).astype(jnp.bfloat16)
    grad_channel = lax.all_to_all(
        grad_conv.T, "sp", split_axis=0, concat_axis=1, tiled=True
    ).astype(jnp.float32)
    padded_grad = jnp.pad(grad_channel, ((0, 0), (0, taps - 1)))
    grad_mixed = jnp.zeros((per_device, full_len), jnp.float32)
    tap_list = []
    for offset in range(taps):
        back = taps - 1 - offset
        grad_mixed = (
            grad_mixed + local_taps[offset][:, None] * padded_grad[:, back : back + full_len]
        )
        tap_list.append(jnp.sum(grad_channel * padded_in[:, offset : offset + full_len], 1))
    back_grad = lax.all_to_all(
        grad_mixed.astype(jnp.bfloat16), "sp", split_axis=1, concat_axis=0, tiled=True
    )
    grad_rows = back_grad.T.astype(jnp.float32)
    grad_taps = lax.all_gather(jnp.stack(tap_list, 0), "sp", axis=1, tiled=True)
    grad_gain = lax.psum(gain_part, "sp")
    grad_val = (grad_rows * sigma_gate).astype(jnp.bfloat16)
    grad_gate = (
        grad_rows * val_input.astype(jnp.float32) * sigma_gate * (1.0 - sigma_gate)
    ).astype(jnp.bfloat16)
    return (grad_val, grad_gate, grad_out_weight, grad_taps, grad_gain)


def solution(mesh):
    in_specs = (P("sp", "dp"), P("sp", "dp"), P("sp", None), P("sp", "dp"), P(None, "dp"), P("dp"))
    out_specs = (P("sp", "dp"), P("sp", "dp"), P("sp", "dp"), P(None, "dp"), P("dp"))
    return jax.shard_map(body, mesh=mesh, in_specs=in_specs, out_specs=out_specs, check_vma=False)
```

profile of v0, /device:TPU:0, one launch (start us, length us, event | category | flops | bytes accessed | tf_op | source)
XLA Modules:
  0.0 334.6 jit_solution(16834628934960173645)
XLA Ops:
  7.9 1.1 fusion.47
  9.1 0.8 copy.22
  9.9 8.3 %all-to-all-start = ((bf16[16,48,128]{2,1,0:T(8,128)(2,1)}), bf16[16,48,128]{2,1,0:T(8,128)(2,1)S(1)}, u32[]{:S(2)}, u32[]{:S(2)}) async-start(bf16[16,48,128]{2,1,0:T(8,128)(2,1)} %bitcast.2), calls=%async_computation | async-start | bytes 393216 | tf_op jit(solution)/shard_map/all_to_all | solution.py:24
  18.3 1.1 dynamic-slice_bitcast_fusion.29
  19.4 1.5 dynamic-slice_bitcast_fusion.30
  20.8 6.0 %all-to-all-done = bf16[16,48,128]{2,1,0:T(8,128)(2,1)S(1)} async-done(((bf16[16,48,128]{2,1,0:T(8,128)(2,1)}), bf16[16,48,128]{2,1,0:T(8,128)(2,1)S(1)}, u32[]{:S(2)}, u32[]{:S(2)}) %all-to-all-start) | async-done | bytes 196640 | tf_op jit(solution)/shard_map/all_to_all | solution.py:24
  26.9 3.5 %copy_bitcast_fusion.3 = bf16[48,16,128]{2,0,1:T(8,128)(2,1)S(1)} fusion(f32[48,2048]{1,0:T(8,128)S(1)} %copy_bitcast_fusion.1, f32[48]{0:T(128)S(1)} %get-tuple-element.91, f32[48]{0:T(128)S(1)} %get-tuple-element.62, f32[48]{0:T(128)S(1)} %get-tuple-element.63, f32[48]{0:T(128)S(1)} %get-tuple-element.64, f32[48]{0:T(128)S(1)} %get-tuple-element.65, ...), kind=kLoop, calls=%fused_computation.118 | loop fusion | flops 6094848 | bytes 595776 | tf_op jit(solution)/shard_map/all_to_all | solution.py:30
  30.4 11.3 %all_to_all.52 = bf16[48,16,128]{2,0,1:T(8,128)(2,1)S(1)} all-to-all(bf16[48,16,128]{2,0,1:T(8,128)(2,1)S(1)} %copy_bitcast_fusion.3), channel_id=1, replica_groups=mesh['sp'=16,'dp'=2] {'sp'}, dimensions={1} | all-to-all | bytes 393216 | tf_op jit(solution)/shard_map/all_to_all | solution.py:30
  42.1 2.5 all-reduce.3
  44.6 7.2 %convolution_bitcast_fusion = f32[4096,768]{0,1:T(8,128)} fusion(bf16[128,4096]{1,0:T(8,128)(2,1)S(1)} %copy-done, f32[768,128]{0,1:T(8,128)S(1)} %copy.25, f32[768]{0:T(1024)} %param.11, f32[128]{0:T(128)S(1)} %get-tuple-element.93, f32[128]{0:T(128)S(1)} %get-tuple-element.92), kind=kOutput, calls=%fused_computation | convolution fusion | flops 806092800 | bytes 14028800 | tf_op jit(solution)/shard_map/dot_general | solution.py:44
  51.8 55.7 %all-gather.3.cloned.1.call-done = bf16[4096,768]{1,0:T(8,128)(2,1)} async-done(((bf16[256,768]{1,0:T(8,128)(2,1)}), bf16[4096,768]{1,0:T(8,128)(2,1)}) %all-gather.3.cloned.1.call-update) | async-done | bytes 6291472 | tf_op jit(solution)/shard_map/all_gather | solution.py:16
  107.5 4.0 %fusion.7 = (f32[768]{0:T(1024)S(1)}, f32[128]{0:T(128)S(1)}, f32[128]{0:T(128)S(1)}, f32[128,768]{1,0:T(8,128)S(1)}) fusion(f32[768,128]{0,1:T(8,128)S(1)} %copy.25, f32[128]{0:T(128)S(1)} %get-tuple-element.93, f32[128]{0:T(128)S(1)} %get-tuple-element.92, f32[768]{0:T(1024)S(1)} %copy-done.3, bf16[128,4096]{1,0:T(8,128)(2,1)S(1)} %copy-done, ...), kind=kOutput, calls=%fused_computation.19 | convolution fusion | flops 806976512 | bytes 8134656 | tf_op jit(solution)/shard_map/dot_general | solution.py:14
  111.5 2.5 all-reduce.2
  114.4 0.8 copy.26
  115.2 4.2 %all-to-all-start.2 = ((bf16[16,48,128]{2,1,0:T(8,128)(2,1)}), bf16[16,48,128]{2,1,0:T(8,128)(2,1)S(1)}, u32[]{:S(2)}, u32[]{:S(2)}) async-start(bf16[16,48,128]{2,1,0:T(8,128)(2,1)} %bitcast.39), calls=%async_computation.2 | async-start | bytes 393216 | tf_op jit(solution)/shard_map/all_to_all | solution.py:58
  119.3 44.3 %psum.39 = f32[768]{0:T(1024)} all-reduce(f32[768]{0:T(1024)S(1)} %get-tuple-element.20), channel_id=1, replica_groups=mesh['sp'=16,'dp'=2] {'sp'}, use_global_device_ids=true, to_apply=%region_41.42 | all-reduce | flops 768 | bytes 6144 | tf_op jit(solution)/shard_map/psum | solution.py:75
  163.7 4.1 %copy_bitcast_fusion.2 = bf16[48,16,128]{2,0,1:T(8,128)(2,1)} fusion(f32[48,2048]{1,0:T(8,128)S(1)} %copy_bitcast_fusion, f32[48]{0:T(128)S(1)} %get-tuple-element.91, f32[48]{0:T(128)S(1)} %get-tuple-element.62, f32[48]{0:T(128)S(1)} %get-tuple-element.63, f32[48]{0:T(128)S(1)} %get-tuple-element.64, f32[48]{0:T(128)S(1)} %get-tuple-element.65, ...), kind=kLoop, calls=%fused_computation.117 | loop fusion | flops 6094848 | bytes 595776 | tf_op jit(solution)/shard_map/all_to_all | solution.py:70
  167.8 3.7 %all-to-all-start.3 = ((bf16[48,16,128]{2,0,1:T(8,128)(2,1)}), bf16[48,16,128]{2,0,1:T(8,128)(2,1)S(1)}, u32[]{:S(2)}, u32[]{:S(2)}) async-start(bf16[48,16,128]{2,0,1:T(8,128)(2,1)} %copy_bitcast_fusion.2), calls=%async_computation.3 | async-start | bytes 393216 | tf_op jit(solution)/shard_map/all_to_all | solution.py:70
  171.5 1.7 multiply_reduce_fusion.1
  173.3 2.5 multiply_reduce_fusion
  175.9 43.4 %all-gather = f32[16,48,31]{1,2,0:T(8,128)S(1)} all-gather(f32[1,48,31]{1,2,0:T(8,128)S(1)} %bitcast.234), channel_id=1, replica_groups=mesh['sp'=16,'dp'=2] {'sp'}, dimensions={0}, use_global_device_ids=true | all-gather | bytes 101184 | tf_op jit(solution)/shard_map/all_gather | solution.py:74
  220.5 0.9 fusion.3
  221.4 104.1 %reduce-scatter.2.cloned.1.call-done = f32[256,768]{0,1:T(8,128)} async-done(((f32[4096,768]{0,1:T(8,128)}), f32[256,768]{0,1:T(8,128)}) %reduce-scatter.2.cloned.1.call-update) | async-done | bytes 786448 | tf_op jit(solution)/shard_map/reduce_scatter | solution.py:43
  325.5 2.3 copy.31
  (28 shorter events, 3.0 us)
Async XLA Ops:
  7.2 37.4 %copy-start = (bf16[128,4096]{1,0:T(8,128)(2,1)S(1)}, bf16[128,4096]{1,0:T(8,128)(2,1)}, u32[]{:S(2)}) copy-start(bf16[128,4096]{1,0:T(8,128)(2,1)} %param.8) | copy-start | bytes 3145732
  7.2 100.3 %all-gather.3.cloned.1.call-start = ((), (), s32[]{:S(2)}) async-start(), calls=%async_computation.5 | async-start | bytes 6684672 | tf_op jit(solution)/shard_map/all_gather | solution.py:16
  9.9 17.0 %all-to-all-start = ((bf16[16,48,128]{2,1,0:T(8,128)(2,1)}), bf16[16,48,128]{2,1,0:T(8,128)(2,1)S(1)}, u32[]{:S(2)}, u32[]{:S(2)}) async-start(bf16[16,48,128]{2,1,0:T(8,128)(2,1)} %bitcast.2), calls=%async_computation | async-start | bytes 393216 | tf_op jit(solution)/shard_map/all_to_all | solution.py:24
  18.2 307.3 %reduce-scatter.2.cloned.1.call-start = ((), (), s32[]{:S(2)}) async-start(), calls=%async_computation.6 | async-start | bytes 13369344 | tf_op jit(solution)/shard_map/reduce_scatter | solution.py:43
  51.8 55.7 %copy-start.3 = (f32[768]{0:T(1024)S(1)}, f32[768]{0:T(1024)}, u32[]{:S(2)}) copy-start(f32[768]{0:T(1024)} %param.11) | copy-start | bytes 9220
  51.8 168.7 %copy-start.1 = (bf16[128,768]{1,0:T(8,128)(2,1)S(1)}, bf16[128,768]{1,0:T(8,128)(2,1)}, u32[]{:S(2)}) copy-start(bf16[128,768]{1,0:T(8,128)(2,1)} %param.6) | copy-start | bytes 589828
  51.8 168.7 %copy-start.2 = (bf16[128,768]{1,0:T(8,128)(2,1)S(1)}, bf16[128,768]{1,0:T(8,128)(2,1)}, u32[]{:S(2)}) copy-start(bf16[128,768]{1,0:T(8,128)(2,1)} %param.7) | copy-start | bytes 589828
  115.2 48.5 %all-to-all-start.2 = ((bf16[16,48,128]{2,1,0:T(8,128)(2,1)}), bf16[16,48,128]{2,1,0:T(8,128)(2,1)S(1)}, u32[]{:S(2)}, u32[]{:S(2)}) async-start(bf16[16,48,128]{2,1,0:T(8,128)(2,1)} %bitcast.39), calls=%async_computation.2 | async-start | bytes 393216 | tf_op jit(solution)/shard_map/all_to_all | solution.py:58
  167.8 52.5 %all-to-all-start.3 = ((bf16[48,16,128]{2,0,1:T(8,128)(2,1)}), bf16[48,16,128]{2,0,1:T(8,128)(2,1)S(1)}, u32[]{:S(2)}, u32[]{:S(2)}) async-start(bf16[48,16,128]{2,0,1:T(8,128)(2,1)} %copy_bitcast_fusion.2), calls=%async_computation.3 | async-start | bytes 393216 | tf_op jit(solution)/shard_map/all_to_all | solution.py:70
Sparse Core Ops, SparseCore 0:
  10.8 96.7 all-gather.2
  113.2 212.2 reduce-scatter.1
where the time goes:
time: 335 us
  waiting for transfers between devices  166 us (50%)
  blocking collectives  104 us (31%)
  starting transfers between devices  16.3 us (5%)
  other arithmetic  14.7 us (4%)
  between operations  14.2 us (4%)
  matrix products  11.2 us (3%)
  local copies, waits for them, and re-layouts  7.86 us (2%)
    reduce_scatter x1, waiting for transfers between devices, body(): lax.psum_scatter(lax.dot_general(columns, swished, (((0,), (0,)), ((), ()...  104 us
    all_gather x1, waiting for transfers between devices, body(): lax.all_gather(out_weight, 'sp', axis=0, tiled=True)  55.7 us
    psum x1, blocking collectives, body(): grad_gain = lax.psum(gain_part, 'sp')  44.3 us
    all_gather x1, blocking collectives, body(): grad_taps = lax.all_gather(jnp.stack(tap_list, 0), 'sp', axis=1, tiled=True)  43.4 us
    all_to_all x1, blocking collectives, body(): lax.all_to_all(conv_out.astype(jnp.bfloat16), 'sp', split_axis=1, concat_...  11.3 us
    all_to_all x1, starting transfers between devices, body(): lax.all_to_all(mixed_in.T, 'sp', split_axis=0, concat_axis=1, tiled=True)  8.34 us
    dot_general x1, matrix products, body(): lax.dot_general(columns, swished, (((0,), (0,)), ((), ())), preferred_ele...  7.21 us
  transfers between devices with their start and end apart: 5, of which 3 were waited for; matrix products, arithmetic and copies ran while one was open for 9% of the time, Pallas kernels for 0%

commit v1 on v0

v1 whole, which is shorter than its diff:
```python
import functools

import jax
import jax.numpy as jnp
from jax import lax
from jax.experimental import pallas as pl
from jax.experimental.pallas import tpu as pltpu
from jax.sharding import PartitionSpec as P

norm_floor = 0.25
F32 = jnp.float32
BF16 = jnp.bfloat16
LOW = 4


def kernel(dims, val, gate, cot, w, taps, gain, gv, gg, gw, gt,
           pin, gcp, nrm, dact, cbuf, sgm, acc1, acc2, inv,
           hs1, hr1, hs2, hr2, cotg, wg, swg, own_mix, mixs, mixr, own_gw, gws, gwr,
           ps1, pr1, ps2, pr2, red, r1, r2, gts,
           h1, h2, cs, cr, fs, fr, ws, wr, p1s, p1r, p2s, p2r, ss, sr, ms, mr, gs, gr,
           t1s, t1r, t2s, t2r, t3s, t3r):
    a, b, dp = dims
    sp = a * b
    tokens, width = val.shape
    taps_n = taps.shape[0]
    channels = width * dp
    chunks, halo_len, tw = pin.shape
    halo = halo_len - tokens
    base = halo - (taps_n - 1)
    rows_w = w.shape[0]
    depth = cotg.shape[1]
    part_t = tokens // dp
    rows_r = red.shape[0] // a

    s = lax.axis_index("sp")
    c = lax.axis_index("dp")
    hi = s // a
    lo = lax.rem(s, a)

    def hi_peer(j):
        return (lax.rem(hi + j, b) * a + lo, c)

    def lo_peer(j):
        return (hi * a + lax.rem(lo + j, a), c)

    def dp_peer(j):
        return (s, lax.rem(c + j, dp))

    after = (lax.rem(s + 1, sp), c)
    before = (lax.rem(s + sp - 1, sp), c)

    def remote(src, dst, send, recv, to):
        return pltpu.make_async_remote_copy(
            src_ref=src, dst_ref=dst, send_sem=send, recv_sem=recv,
            device_id=to, device_id_type=pl.DeviceIdType.MESH)

    def lanes(i):
        if chunks == 1:
            return pl.ds(0, tw)
        return pl.ds(pl.multiple_of(i * tw, tw), tw)

    barrier = pltpu.get_barrier_semaphore()
    peers = ([after, before] + [hi_peer(j) for j in range(1, b)]
             + [lo_peer(j) for j in range(1, a)] + [dp_peer(j) for j in range(1, dp)])
    for peer in peers:
        pl.semaphore_signal(barrier, inc=1, device_id=peer, device_id_type=pl.DeviceIdType.MESH)

    @pl.loop(0, chunks)
    def _(i):
        at = lanes(i)
        sig = jax.nn.sigmoid(gate[:, at].astype(F32))
        sgm[i] = sig
        mixed = (val[:, at].astype(F32) * sig).astype(BF16)
        hs1[:, at] = mixed[tokens - halo:]
        pin[i, halo:, :] = mixed.astype(F32)

    pl.semaphore_wait(barrier, len(peers))

    sends = []
    halo1 = remote(hs1, hr1, h1.at[0], h1.at[1], after)
    halo1.start()
    my_rows = pl.ds(pl.multiple_of(c * part_t, part_t), part_t)
    cot_in = []
    for j in range(1, b):
        other = lax.rem(hi + j, b)
        copy = remote(cot.at[my_rows, pl.ds(pl.multiple_of(other * depth, 128), depth)],
                      cotg.at[pl.ds(pl.multiple_of(hi * tokens + c * part_t, part_t), part_t), :],
                      cs.at[j - 1], cr.at[j - 1], hi_peer(j))
        copy.start()
        cot_in.append(copy)
    w_in = []
    for j in range(1, a):
        copy = remote(w, wg.at[pl.ds(pl.multiple_of(lo * rows_w, rows_w), rows_w), :],
                      ws.at[j - 1], wr.at[j - 1], lo_peer(j))
        copy.start()
        w_in.append(copy)
    own_rows = pl.ds(pl.multiple_of(hi * tokens, tokens), tokens)
    cotg[own_rows, :] = cot[:, pl.ds(pl.multiple_of(hi * depth, 128), depth)]
    wg[pl.ds(pl.multiple_of(lo * rows_w, rows_w), rows_w), :] = w[...]
    sends += [halo1] + cot_in + w_in

    halo1.wait_recv()
    keep_first = (s > 0).astype(F32)
    acc1[...] = jnp.zeros_like(acc1)
    acc2[...] = jnp.zeros_like(acc2)

    @pl.loop(0, chunks)
    def _(i):
        at = lanes(i)
        pin[i, :halo, :] = hr1[:, at].astype(F32) * keep_first
        total = jnp.zeros((tokens, tw), F32)
        for k in range(taps_n):
            total = total + taps[k:k + 1, at] * pin[i, base + k:base + k + tokens, :]
        rounded = total.astype(BF16).astype(F32)
        cbuf[i] = rounded
        acc1[...] += rounded
        acc2[...] += rounded * rounded

    def share(buf, got, send, recv):
        buf[0] = jnp.broadcast_to(jnp.sum(acc1[...], 1, keepdims=True), (tokens, tw))
        buf[1] = jnp.broadcast_to(jnp.sum(acc2[...], 1, keepdims=True), (tokens, tw))
        copies = []
        for j in range(1, dp):
            copy = remote(buf, got.at[j - 1], send.at[j - 1], recv.at[j - 1], dp_peer(j))
            copy.start()
            copies.append(copy)
        return copies

    def gathered(buf, got, copies):
        for copy in copies:
            copy.wait_recv()
        for j in range(1, dp):
            buf_sum = got[j - 1]
            acc1[...] = (buf[0] if j == 1 else acc1[...]) + buf_sum[0]
            acc2[...] = (buf[1] if j == 1 else acc2[...]) + buf_sum[1]

    first = share(ps1, pr1, p1s, p1r)
    gathered(ps1, pr1, first)
    sends += first
    mean = acc1[...] / channels
    inv[...] = lax.rsqrt(acc2[...] / channels - mean * mean + norm_floor)
    acc1[...] = mean

    @pl.loop(0, chunks)
    def _(i):
        at = lanes(i)
        normed = (cbuf[i] - acc1[...]) * inv[...]
        act = normed * gain[:, at]
        sig = jax.nn.sigmoid(act)
        swg[own_rows, at] = (act * sig).astype(BF16)
        nrm[i] = normed
        dact[i] = sig * (1.0 + act * (1.0 - sig))

    sw_in = []
    for j in range(1, b):
        copy = remote(swg.at[own_rows, :], swg.at[own_rows, :], ss.at[j - 1], sr.at[j - 1], hi_peer(j))
        copy.start()
        sw_in.append(copy)
    sends += sw_in

    forwards = []
    for j in range(1, b):
        cot_in[j - 1].wait_recv()
        origin = lax.rem(hi + b - j, b)
        rows = cotg.at[pl.ds(pl.multiple_of(origin * tokens + c * part_t, part_t), part_t), :]
        for d in range(1, dp):
            copy = remote(rows, rows, fs.at[j - 1, d - 1], fr.at[j - 1, d - 1], dp_peer(d))
            copy.start()
            forwards.append(copy)
    for copy in w_in + forwards:
        copy.wait_recv()
    sends += forwards

    def mix_copy(j):
        return remote(mixs.at[j - 1], mixr.at[j - 1], ms.at[j - 1], mr.at[j - 1], hi_peer(j))

    @pl.loop(1, b)
    def _(j):
        other = lax.rem(hi + j, b)
        block = cotg[pl.ds(pl.multiple_of(other * tokens, tokens), tokens), :]
        mixs[j - 1] = jnp.dot(block, wg[...], preferred_element_type=F32).astype(BF16)
        mix_copy(j).start()

    own_mix[...] = jnp.dot(cotg[own_rows, :], wg[...], preferred_element_type=F32)

    for copy in sw_in:
        copy.wait_recv()

    def gw_copy(q, j):
        return remote(gws.at[q], gwr.at[j - 1], gs.at[j - 1], gr.at[j - 1], (hi * a + q, c))

    for q in range(a):
        part = lax.dot_general(cotg[:, q * rows_w:(q + 1) * rows_w], swg[...],
                               (((0,), (0,)), ((), ())), preferred_element_type=F32)

        @pl.when(lo == q)
        def _():
            own_gw[...] = part

        @pl.when(lo != q)
        def _():
            gws[q] = part.astype(BF16)
            gw_copy(q, lax.rem(q - lo + a, a)).start()

    for j in range(1, b):
        mix_copy(j).wait_recv()
    acc1[...] = jnp.zeros_like(acc1)
    acc2[...] = jnp.zeros_like(acc2)
    red[...] = jnp.zeros_like(red)

    @pl.loop(0, chunks)
    def _(i):
        at = lanes(i)
        mix = own_mix[:, at]
        for j in range(1, b):
            mix = mix + mixr[j - 1, :, at].astype(F32)
        grad_act = mix * dact[i]
        normed = nrm[i]
        red[taps_n:taps_n + 1, at] = jnp.sum(grad_act * normed, 0, keepdims=True)
        grad_norm = grad_act * gain[:, at]
        cbuf[i] = grad_norm
        acc1[...] += grad_norm
        acc2[...] += grad_norm * normed

    second = share(ps2, pr2, p2s, p2r)
    gathered(ps2, pr2, second)
    sends += second
    acc1[...] = acc1[...] / channels
    acc2[...] = acc2[...] / channels

    @pl.loop(0, chunks)
    def _(i):
        at = lanes(i)
        rounded = (inv[...] * (cbuf[i] - acc1[...] - nrm[i] * acc2[...])).astype(BF16)
        hs2[:, at] = rounded[:halo]
        gcp[i, :tokens, :] = rounded.astype(F32)

    halo2 = remote(hs2, hr2, h2.at[0], h2.at[1], before)
    halo2.start()
    sends.append(halo2)

    @pl.loop(0, chunks)
    def _(i):
        at = lanes(i)
        grad = gcp[i, :tokens, :]
        for k in range(taps_n):
            red[k:k + 1, at] = jnp.sum(grad * pin[i, base + k:base + k + tokens, :], 0, keepdims=True)

    stage1 = []
    for j in range(1, a):
        other = lax.rem(lo + j, a)
        copy = remote(red.at[pl.ds(pl.multiple_of(other * rows_r, 8), rows_r), :], r1.at[j - 1],
                      t1s.at[j - 1], t1r.at[j - 1], lo_peer(j))
        copy.start()
        stage1.append(copy)
    sends += stage1

    halo2.wait_recv()
    keep_last = (s < sp - 1).astype(F32)

    @pl.loop(0, chunks)
    def _(i):
        at = lanes(i)
        gcp[i, tokens:, :] = hr2[:, at].astype(F32) * keep_last
        total = jnp.zeros((tokens, tw), F32)
        for k in range(taps_n):
            back = taps_n - 1 - k
            total = total + taps[k:k + 1, at] * gcp[i, back:back + tokens, :]
        grad = total.astype(BF16).astype(F32)
        sig = sgm[i]
        gv[:, at] = (grad * sig).astype(BF16)
        gg[:, at] = (grad * val[:, at].astype(F32) * sig * (1.0 - sig)).astype(BF16)

    for copy in stage1:
        copy.wait_recv()
    mine = red[pl.ds(pl.multiple_of(lo * rows_r, 8), rows_r), :]
    for j in range(1, a):
        mine = mine + r1[j - 1]
    r2[hi] = mine
    stage2 = []
    for j in range(1, b):
        copy = remote(r2.at[hi], r2.at[hi], t2s.at[j - 1], t2r.at[j - 1], hi_peer(j))
        copy.start()
        stage2.append(copy)
    sends += stage2
    for copy in stage2:
        copy.wait_recv()
    summed = r2[0]
    for j in range(1, b):
        summed = summed + r2[j]
    my_red = pl.ds(pl.multiple_of(lo * rows_r, 8), rows_r)
    gts[my_red, :] = summed
    stage3 = []
    for j in range(1, a):
        copy = remote(gts.at[my_red, :], gts.at[my_red, :], t3s.at[j - 1], t3r.at[j - 1], lo_peer(j))
        copy.start()
        stage3.append(copy)
    sends += stage3

    for j in range(1, a):
        gw_copy(0, j).wait_recv()
    total = own_gw[...]
    for j in range(1, a):
        total = total + gwr[j - 1].astype(F32)
    gw[...] = total

    for copy in stage3:
        copy.wait_recv()
    gt[...] = gts[...]

    for copy in sends:
        copy.wait_send()
    for j in range(1, b):
        mix_copy(j).wait_send()
    for j in range(1, a):
        gw_copy(0, j).wait_send()


def body(sp, dp, val, gate, cot, w, taps, gain):
    a = LOW if sp % LOW == 0 else 1
    b = sp // a
    tokens, width = val.shape
    rows_w = w.shape[0]
    model = cot.shape[1]
    depth = model // b
    taps_n = taps.shape[0]
    tw = 128 if width % 128 == 0 else width
    chunks = width // tw
    halo = -(-(taps_n - 1) // 16) * 16
    rows = -(-(taps_n + 1) // (8 * a)) * 8 * a
    vm, dma = pltpu.VMEM, pltpu.SemaphoreType.DMA
    scratch = [
        vm((chunks, tokens + halo, tw), F32),
        vm((chunks, tokens + halo, tw), F32),
        vm((chunks, tokens, tw), F32),
        vm((chunks, tokens, tw), F32),
        vm((chunks, tokens, tw), F32),
        vm((chunks, tokens, tw), F32),
        vm((tokens, tw), F32),
        vm((tokens, tw), F32),
        vm((tokens, tw), F32),
        vm((halo, width), BF16),
        vm((halo, width), BF16),
        vm((halo, width), BF16),
        vm((halo, width), BF16),
        vm((b * tokens, depth), BF16),
        vm((depth, width), BF16),
        vm((b * tokens, width), BF16),
        vm((tokens, width), F32),
        vm((b - 1, tokens, width), BF16),
        vm((b - 1, tokens, width), BF16),
        vm((rows_w, width), F32),
        vm((a, rows_w, width), BF16),
        vm((a - 1, rows_w, width), BF16),
        vm((2, tokens, tw), F32),
        vm((dp - 1, 2, tokens, tw), F32),
        vm((2, tokens, tw), F32),
        vm((dp - 1, 2, tokens, tw), F32),
        vm((rows, width), F32),
        vm((a - 1, rows // a, width), F32),
        vm((b, rows // a, width), F32),
        vm((rows, width), F32),
        dma((2,)), dma((2,)),
        dma((b - 1,)), dma((b - 1,)),
        dma((b - 1, dp - 1)), dma((b - 1, dp - 1)),
        dma((a - 1,)), dma((a - 1,)),
        dma((dp - 1,)), dma((dp - 1,)), dma((dp - 1,)), dma((dp - 1,)),
        dma((b - 1,)), dma((b - 1,)),
        dma((b - 1,)), dma((b - 1,)),
        dma((a - 1,)), dma((a - 1,)),
        dma((a - 1,)), dma((a - 1,)),
        dma((b - 1,)), dma((b - 1,)),
        dma((a - 1,)), dma((a - 1,)),
    ]
    spec = pl.BlockSpec(memory_space=pltpu.VMEM)
    gv, gg, gw, gt = pl.pallas_call(
        functools.partial(kernel, (a, b, dp)),
        out_shape=(
            jax.ShapeDtypeStruct((tokens, width), BF16),
            jax.ShapeDtypeStruct((tokens, width), BF16),
            jax.ShapeDtypeStruct((rows_w, width), F32),
            jax.ShapeDtypeStruct((rows, width), F32),
        ),
        in_specs=[spec] * 6,
        out_specs=(spec,) * 4,
        scratch_shapes=scratch,
        compiler_params=pltpu.CompilerParams(
            collective_id=0, has_side_effects=True, vmem_limit_bytes=56 * 1024 * 1024),
    )(val, gate, cot, w, taps, gain[None, :])
    return gv, gg, gw, gt[:taps_n], gt[taps_n]


def solution(mesh):
    in_specs = (P("sp", "dp"), P("sp", "dp"), P("sp", None), P("sp", "dp"), P(None, "dp"), P("dp"))
    out_specs = (P("sp", "dp"), P("sp", "dp"), P("sp", "dp"), P(None, "dp"), P("dp"))
    run = functools.partial(body, mesh.shape["sp"], mesh.shape["dp"])
    return jax.shard_map(run, mesh=mesh, in_specs=in_specs, out_specs=out_specs, check_vma=False)
```

time: 335 us -> 84.3 us (0.25)
  waiting for transfers between devices: 166 us -> 0 us
  blocking collectives: 104 us -> 0 us
  Pallas kernels: 0 us -> 75.8 us
  starting transfers between devices: 16.3 us -> 0 us
  other arithmetic: 14.7 us -> 0 us
  between operations: 14.2 us -> 0.65 us
  matrix products: 11.2 us -> 0 us
    reduce_scatter x1 -> x0, waiting for transfers between devices: 104 us -> none  [body(): lax.psum_scatter(lax.dot_general(columns, swished, (((0,), (0,)), ((), ()...]
    pallas_call x0 -> x1, Pallas kernels: none -> 75.8 us  [body(): pl.pallas_call(functools.partial(kernel, (a, b, dp)), out_shape=(jax.Shap...]
    all_gather x1 -> x0, waiting for transfers between devices: 55.7 us -> none  [body(): lax.all_gather(out_weight, 'sp', axis=0, tiled=True)]
    psum x3 -> x0, blocking collectives: 49.2 us -> none  [the longest x1 44.3 us: body(): grad_gain = lax.psum(gain_part, 'sp')]
    all_gather x1 -> x0, blocking collectives: 43.4 us -> none  [body(): grad_taps = lax.all_gather(jnp.stack(tap_list, 0), 'sp', axis=1, tiled=True)]
    all_to_all x3 -> x0, starting transfers between devices: 16.2 us -> none  [the longest x1 8.34 us: body(): lax.all_to_all(mixed_in.T, 'sp', split_axis=0, concat_axis=1, tiled=True)]
    all_to_all x1 -> x0, blocking collectives: 11.3 us -> none  [body(): lax.all_to_all(conv_out.astype(jnp.bfloat16), 'sp', split_axis=1, concat_...]
    dot_general x2 -> x0, matrix products: 11.2 us -> none  [the longest x1 7.21 us: body(): lax.dot_general(columns, swished, (((0,), (0,)), ((), ())), preferred_ele...]
  transfers between devices with their start and end apart: 5 -> 0, of which waited for: 3 -> 0; matrix products, arithmetic and copies ran while one was open for 9% -> 0% of each run, Pallas kernels for 0% -> 0%
where the time goes in v1:
time: 84.3 us; the launch traced here: 84 us
  Pallas kernels  75.8 us (90%)
  local copies, waits for them, and re-layouts  7.52 us (9%)
    pallas_call x1, Pallas kernels, body(): pl.pallas_call(functools.partial(kernel, (a, b, dp)), out_shape=(jax.Shap...  75.8 us
    unnamed x8, local copies, waits for them, and re-layouts  4.84 us

profile of v1, /device:TPU:0, one launch (start us, length us, event | category | flops | bytes accessed | tf_op | source)
XLA Modules:
  0.0 84.0 jit_solution(18299276954868004290)
XLA Ops:
  0.6 1.3 %broadcast_in_dim.3.gain = f32[1,768]{1,0:T(1,128)} reshape(f32[768]{0:T(1024)} %param.11) | data formatting | bytes 6144 | tf_op jit(solution)/shard_map/broadcast_in_dim | solution.py:389
  1.9 75.8 %shard_map.101 = (bf16[128,768]{1,0:T(8,128)(2,1)}, bf16[128,768]{1,0:T(8,128)(2,1)}, f32[256,768]{1,0:T(8,128)}, f32[32,768]{1,0:T(8,128)}) custom-call(bf16[128,768]{1,0:T(8,128)(2,1)} %val.1, bf16[128,768]{1,0:T(8,128)(2,1)} %gate.1, bf16[128,4096]{1,0:T(8,128)(2,1)} %cot.1, bf16[256,768]{1,0:T(8,128)(2,1)} %w.1, f32[31,768]{1,0:T(8,128)} %taps.1, ...), custom_call_target="tpu_custom_call" | custom-call | tf_op jit(solution)/shard_map/pallas_call | solution.py:376
  77.7 0.0 copy-start
  77.7 1.4 %slice_reduce_fusion = f32[768]{0:T(1024)} fusion(f32[32,768]{1,0:T(8,128)} %get-tuple-element.12), kind=kLoop, calls=%fused_computation | loop fusion | bytes 6144 | tf_op jit(solution)/shard_map/slice | solution.py:390
  79.1 1.6 %copy.15 = bf16[128,768]{1,0:T(8,128)(2,1)} copy(bf16[128,768]{1,0:T(8,128)(2,1)} %get-tuple-element.18) | data formatting | bytes 393216
  80.8 1.6 %copy.16 = bf16[128,768]{1,0:T(8,128)(2,1)} copy(bf16[128,768]{1,0:T(8,128)(2,1)} %get-tuple-element.19) | data formatting | bytes 393216
  82.4 0.0 copy-done
  82.4 0.0 copy-start.1
  82.4 0.9 %copy.17 = f32[256,768]{1,0:T(8,128)} copy(f32[256,768]{1,0:T(8,128)S(1)} %copy-done) | data formatting | bytes 1572864
  83.3 0.1 copy-done.1
  83.3 0.6 copy.18
Async XLA Ops:
  77.7 4.7 %copy-start = (f32[256,768]{1,0:T(8,128)S(1)}, f32[256,768]{1,0:T(8,128)}, u32[]{:S(2)}) copy-start(f32[256,768]{1,0:T(8,128)} %get-tuple-element.20) | copy-start | bytes 2359300
  82.4 1.0 %copy-start.1 = (f32[32,768]{1,0:T(8,128)S(1)}, f32[32,768]{1,0:T(8,128)}, u32[]{:S(2)}) copy-start(f32[32,768]{1,0:T(8,128)} %get-tuple-element.12) | copy-start | bytes 294916

commit v2 on v1

--- a/solution.py
+++ b/solution.py
@@ -13,8 +13,8 @@
 LOW = 4
 
 
-def kernel(dims, val, gate, cot, w, taps, gain, gv, gg, gw, gt,
-           pin, gcp, nrm, dact, cbuf, sgm, acc1, acc2, inv,
+def kernel(dims, val_in, gate_in, cot, w, taps, gain, gv, gg, gw, gt,
+           val, gate, loads, cott, pin, gcp, nrm, dact, cbuf, sgm, acc1, acc2, inv,
            hs1, hr1, hs2, hr2, cotg, wg, swg, own_mix, mixs, mixr, own_gw, gws, gwr,
            ps1, pr1, ps2, pr2, red, r1, r2, gts,
            h1, h2, cs, cr, fs, fr, ws, wr, p1s, p1r, p2s, p2r, ss, sr, ms, mr, gs, gr,
@@ -29,6 +29,8 @@
     base = halo - (taps_n - 1)
     rows_w = w.shape[0]
     depth = cotg.shape[1]
+    parts, _, wp = wg.shape
+    per = chunks // parts
     part_t = tokens // dp
     rows_r = red.shape[0] // a
 
@@ -59,11 +61,29 @@
             return pl.ds(0, tw)
         return pl.ds(pl.multiple_of(i * tw, tw), tw)
 
+    def place(i):
+        if parts == 1:
+            return 0, lanes(i)
+        return i // per, pl.ds(pl.multiple_of(lax.rem(i, per) * tw, tw), tw)
+
+    own_rows = pl.ds(pl.multiple_of(hi * tokens, tokens), tokens)
+    own_depth = pl.ds(pl.multiple_of(lo * rows_w, rows_w), rows_w)
     barrier = pltpu.get_barrier_semaphore()
     peers = ([after, before] + [hi_peer(j) for j in range(1, b)]
              + [lo_peer(j) for j in range(1, a)] + [dp_peer(j) for j in range(1, dp)])
     for peer in peers:
         pl.semaphore_signal(barrier, inc=1, device_id=peer, device_id_type=pl.DeviceIdType.MESH)
+
+    local = [pltpu.make_async_copy(val_in, val, loads.at[0]),
+             pltpu.make_async_copy(gate_in, gate, loads.at[1]),
+             pltpu.make_async_copy(cot.at[:, pl.ds(pl.multiple_of(hi * depth, 128), depth)],
+                                   cotg.at[own_rows, :], loads.at[2])]
+    for h in range(parts):
+        local.append(pltpu.make_async_copy(w.at[:, h * wp:(h + 1) * wp], wg.at[h, own_depth, :], loads.at[3 + h]))
+    for copy in local:
+        copy.start()
+    local[0].wait()
+    local[1].wait()
 
     @pl.loop(0, chunks)
     def _(i):
@@ -88,16 +108,14 @@
                       cs.at[j - 1], cr.at[j - 1], hi_peer(j))
         copy.start()
         cot_in.append(copy)
-    w_in = []
-    for j in range(1, a):
-        copy = remote(w, wg.at[pl.ds(pl.multiple_of(lo * rows_w, rows_w), rows_w), :],
-                      ws.at[j - 1], wr.at[j - 1], lo_peer(j))
-        copy.start()
-        w_in.append(copy)
-    own_rows = pl.ds(pl.multiple_of(hi * tokens, tokens), tokens)
-    cotg[own_rows, :] = cot[:, pl.ds(pl.multiple_of(hi * depth, 128), depth)]
-    wg[pl.ds(pl.multiple_of(lo * rows_w, rows_w), rows_w), :] = w[...]
-    sends += [halo1] + cot_in + w_in
+    w_in = [[] for _ in range(parts)]
+    for h in range(parts):
+        for j in range(1, a):
+            copy = remote(w.at[:, h * wp:(h + 1) * wp], wg.at[h, own_depth, :],
+                          ws.at[h, j - 1], wr.at[h, j - 1], lo_peer(j))
+            copy.start()
+            w_in[h].append(copy)
+    sends += [halo1] + cot_in + sum(w_in, [])
 
     halo1.wait_recv()
     keep_first = (s > 0).astype(F32)
@@ -145,18 +163,19 @@
     def _(i):
         at = lanes(i)
         normed = (cbuf[i] - acc1[...]) * inv[...]
-        act = normed * gain[:, at]
+        act = normed * gain[at][None, :]
+        part, within = place(i)
         sig = jax.nn.sigmoid(act)
-        swg[own_rows, at] = (act * sig).astype(BF16)
+        swg[part, own_rows, within] = (act * sig).astype(BF16)
         nrm[i] = normed
         dact[i] = sig * (1.0 + act * (1.0 - sig))
 
-    sw_in = []
+    def sw_copy(h, j):
+        return remote(swg.at[h, own_rows, :], swg.at[h, own_rows, :],
+                      ss.at[h, j - 1], sr.at[h, j - 1], hi_peer(j))
+
     for j in range(1, b):
-        copy = remote(swg.at[own_rows, :], swg.at[own_rows, :], ss.at[j - 1], sr.at[j - 1], hi_peer(j))
-        copy.start()
-        sw_in.append(copy)
-    sends += sw_in
+        sw_copy(0, j).start()
 
     forwards = []
     for j in range(1, b):
@@ -167,43 +186,56 @@
             copy = remote(rows, rows, fs.at[j - 1, d - 1], fr.at[j - 1, d - 1], dp_peer(d))
             copy.start()
             forwards.append(copy)
-    for copy in w_in + forwards:
+    sends += forwards
+    for copy in local[2:]:
+        copy.wait()
+    for copy in forwards:
         copy.wait_recv()
-    sends += forwards
-
-    def mix_copy(j):
-        return remote(mixs.at[j - 1], mixr.at[j - 1], ms.at[j - 1], mr.at[j - 1], hi_peer(j))
-
-    @pl.loop(1, b)
-    def _(j):
-        other = lax.rem(hi + j, b)
-        block = cotg[pl.ds(pl.multiple_of(other * tokens, tokens), tokens), :]
-        mixs[j - 1] = jnp.dot(block, wg[...], preferred_element_type=F32).astype(BF16)
-        mix_copy(j).start()
-
-    own_mix[...] = jnp.dot(cotg[own_rows, :], wg[...], preferred_element_type=F32)
-
-    for copy in sw_in:
-        copy.wait_recv()
-
-    def gw_copy(q, j):
-        return remote(gws.at[q], gwr.at[j - 1], gs.at[j - 1], gr.at[j - 1], (hi * a + q, c))
-
+
+    def mix_copy(h, j):
+        return remote(mixs.at[h, j - 1], mixr.at[h, j - 1], ms.at[h, j - 1], mr.at[h, j - 1], hi_peer(j))
+
+    for h in range(parts):
+        for copy in w_in[h]:
+            copy.wait_recv()
+
+        @pl.loop(1, b)
+        def _(j):
+            other = lax.rem(hi + j, b)
+            block = cotg[pl.ds(pl.multiple_of(other * tokens, tokens), tokens), :]
+            mixs[h, j - 1] = jnp.dot(block, wg[h], preferred_element_type=F32).astype(BF16)
+            mix_copy(h, j).start()
+
+    for h in range(1, parts):
+        for j in range(1, b):
+            sw_copy(h, j).start()
+
+    for h in range(parts):
+        own_mix[h] = jnp.dot(cotg[own_rows, :], wg[h], preferred_element_type=F32)
     for q in range(a):
-        part = lax.dot_general(cotg[:, q * rows_w:(q + 1) * rows_w], swg[...],
-                               (((0,), (0,)), ((), ())), preferred_element_type=F32)
-
-        @pl.when(lo == q)
-        def _():
-            own_gw[...] = part
-
-        @pl.when(lo != q)
-        def _():
-            gws[q] = part.astype(BF16)
-            gw_copy(q, lax.rem(q - lo + a, a)).start()
-
-    for j in range(1, b):
-        mix_copy(j).wait_recv()
+        cott[q * rows_w:(q + 1) * rows_w, :] = cotg[:, q * rows_w:(q + 1) * rows_w].T
+
+    def gw_copy(h, j):
+        return remote(gws.at[h, j - 1], gwr.at[h, j - 1], gs.at[h, j - 1], gr.at[h, j - 1], lo_peer(j))
+
+    def gw_part(h):
+        for j in range(1, b):
+            sw_copy(h, j).wait_recv()
+
+        @pl.loop(1, a)
+        def _(j):
+            other = lax.rem(lo + j, a)
+            block = cott[pl.ds(pl.multiple_of(other * rows_w, rows_w), rows_w), :]
+            gws[h, j - 1] = jnp.dot(block, swg[h], preferred_element_type=F32).astype(BF16)
+            gw_copy(h, j).start()
+
+        own_gw[h] = jnp.dot(cott[own_depth, :], swg[h], preferred_element_type=F32)
+
+    gw_part(0)
+
+    for h in range(parts):
+        for j in range(1, b):
+            mix_copy(h, j).wait_recv()
     acc1[...] = jnp.zeros_like(acc1)
     acc2[...] = jnp.zeros_like(acc2)
     red[...] = jnp.zeros_like(red)
@@ -211,13 +243,14 @@
     @pl.loop(0, chunks)
     def _(i):
         at = lanes(i)
-        mix = own_mix[:, at]
+        part, within = place(i)
+        mix = own_mix[part, :, within]
         for j in range(1, b):
-            mix = mix + mixr[j - 1, :, at].astype(F32)
+            mix = mix + mixr[part, j - 1, :, within].astype(F32)
         grad_act = mix * dact[i]
         normed = nrm[i]
         red[taps_n:taps_n + 1, at] = jnp.sum(grad_act * normed, 0, keepdims=True)
-        grad_norm = grad_act * gain[:, at]
+        grad_norm = grad_act * gain[at][None, :]
         cbuf[i] = grad_norm
         acc1[...] += grad_norm
         acc2[...] += grad_norm * normed
@@ -254,6 +287,8 @@
         copy.start()
         stage1.append(copy)
     sends += stage1
+    for h in range(1, parts - 1):
+        gw_part(h)
 
     halo2.wait_recv()
     keep_last = (s < sp - 1).astype(F32)
@@ -283,6 +318,8 @@
         copy.start()
         stage2.append(copy)
     sends += stage2
+    if parts > 1:
+        gw_part(parts - 1)
     for copy in stage2:
         copy.wait_recv()
     summed = r2[0]
@@ -297,12 +334,13 @@
         stage3.append(copy)
     sends += stage3
 
-    for j in range(1, a):
-        gw_copy(0, j).wait_recv()
-    total = own_gw[...]
-    for j in range(1, a):
-        total = total + gwr[j - 1].astype(F32)
-    gw[...] = total
+    for h in range(parts):
+        for j in range(1, a):
+            gw_copy(h, j).wait_recv()
+        total = own_gw[h]
+        for j in range(1, a):
+            total = total + gwr[h, j - 1].astype(F32)
+        gw[:, h * wp:(h + 1) * wp] = total
 
     for copy in stage3:
         copy.wait_recv()
@@ -310,10 +348,21 @@
 
     for copy in sends:
         copy.wait_send()
-    for j in range(1, b):
-        mix_copy(j).wait_send()
-    for j in range(1, a):
-        gw_copy(0, j).wait_send()
+    for h in range(parts):
+        for j in range(1, b):
+            sw_copy(h, j).wait_send()
+            mix_copy(h, j).wait_send()
+        for j in range(1, a):
+            gw_copy(h, j).wait_send()
+
+
+def finish(gv, gg, gw, gt, out_gv, out_gg, out_gw, out_taps, out_gain):
+    out_gv[...] = gv[...]
+    out_gg[...] = gg[...]
+    out_gw[...] = gw[...]
+    taps_n = out_taps.shape[0]
+    out_taps[...] = gt[:taps_n]
+    out_gain[...] = gt[taps_n]
 
 
 def body(sp, dp, val, gate, cot, w, taps, gain):
@@ -328,8 +377,14 @@
     chunks = width // tw
     halo = -(-(taps_n - 1) // 16) * 16
     rows = -(-(taps_n + 1) // (8 * a)) * 8 * a
+    parts = 3 if chunks % 3 == 0 else 2 if chunks % 2 == 0 else 1
+    wp = width // parts
     vm, dma = pltpu.VMEM, pltpu.SemaphoreType.DMA
     scratch = [
+        vm((tokens, width), BF16),
+        vm((tokens, width), BF16),
+        dma((3 + parts,)),
+        vm((depth, b * tokens), BF16),
         vm((chunks, tokens + halo, tw), F32),
         vm((chunks, tokens + halo, tw), F32),
         vm((chunks, tokens, tw), F32),
@@ -344,14 +399,14 @@
         vm((halo, width), BF16),
         vm((halo, width), BF16),
         vm((b * tokens, depth), BF16),
-        vm((depth, width), BF16),
-        vm((b * tokens, width), BF16),
-        vm((tokens, width), F32),
-        vm((b - 1, tokens, width), BF16),
-        vm((b - 1, tokens, width), BF16),
-        vm((rows_w, width), F32),
-        vm((a, rows_w, width), BF16),
-        vm((a - 1, rows_w, width), BF16),
+        vm((parts, depth, wp), BF16),
+        vm((parts, b * tokens, wp), BF16),
+        vm((parts, tokens, wp), F32),
+        vm((parts, b - 1, tokens, wp), BF16),
+        vm((parts, b - 1, tokens, wp), BF16),
+        vm((parts, rows_w, wp), F32),
+        vm((parts, a - 1, rows_w, wp), BF16),
+        vm((parts, a - 1, rows_w, wp), BF16),
         vm((2, tokens, tw), F32),
         vm((dp - 1, 2, tokens, tw), F32),
         vm((2, tokens, tw), F32),
@@ -363,17 +418,18 @@
         dma((2,)), dma((2,)),
         dma((b - 1,)), dma((b - 1,)),
         dma((b - 1, dp - 1)), dma((b - 1, dp - 1)),
-        dma((a - 1,)), dma((a - 1,)),
+        dma((parts, a - 1)), dma((parts, a - 1)),
         dma((dp - 1,)), dma((dp - 1,)), dma((dp - 1,)), dma((dp - 1,)),
-        dma((b - 1,)), dma((b - 1,)),
-        dma((b - 1,)), dma((b - 1,)),
-        dma((a - 1,)), dma((a - 1,)),
+        dma((parts, b - 1)), dma((parts, b - 1)),
+        dma((parts, b - 1)), dma((parts, b - 1)),
+        dma((parts, a - 1)), dma((parts, a - 1)),
         dma((a - 1,)), dma((a - 1,)),
         dma((b - 1,)), dma((b - 1,)),
         dma((a - 1,)), dma((a - 1,)),
     ]
     spec = pl.BlockSpec(memory_space=pltpu.VMEM)
-    gv, gg, gw, gt = pl.pallas_call(
+    anywhere = pl.BlockSpec(memory_space=pl.ANY)
+    results = pl.pallas_call(
         functools.partial(kernel, (a, b, dp)),
         out_shape=(
             jax.ShapeDtypeStruct((tokens, width), BF16),
@@ -381,13 +437,24 @@
             jax.ShapeDtypeStruct((rows_w, width), F32),
             jax.ShapeDtypeStruct((rows, width), F32),
         ),
-        in_specs=[spec] * 6,
+        in_specs=[anywhere] * 4 + [spec] * 2,
         out_specs=(spec,) * 4,
         scratch_shapes=scratch,
         compiler_params=pltpu.CompilerParams(
             collective_id=0, has_side_effects=True, vmem_limit_bytes=56 * 1024 * 1024),
-    )(val, gate, cot, w, taps, gain[None, :])
-    return gv, gg, gw, gt[:taps_n], gt[taps_n]
+    )(val, gate, cot, w, taps, gain)
+    return pl.pallas_call(
+        finish,
+        out_shape=(
+            jax.ShapeDtypeStruct((tokens, width), BF16),
+            jax.ShapeDtypeStruct((tokens, width), BF16),
+            jax.ShapeDtypeStruct((rows_w, width), F32),
+            jax.ShapeDtypeStruct((taps_n, width), F32),
+            jax.ShapeDtypeStruct((width,), F32),
+        ),
+        in_specs=[spec] * 4,
+        out_specs=(spec,) * 5,
+    )(*results)
 
 
 def solution(mesh):

time: 84.3 us -> 70 us (0.83)
  local copies, waits for them, and re-layouts: 7.52 us -> 0 us
  Pallas kernels: 75.8 us -> 68.5 us
    pallas_call x1, Pallas kernels: 75.8 us -> 66.1 us  [body(): pl.pallas_call(functools.partial(kernel, (a, b, dp)), out_shape=(jax.Shap...]
    unnamed x8 -> x0, local copies, waits for them, and re-layouts: 4.84 us -> none
    pallas_call x0 -> x1, Pallas kernels: none -> 2.4 us  [body(): pl.pallas_call(finish, out_shape=(jax.ShapeDtypeStruct((tokens, width), B...]
    slice x1 -> x0, local copies, waits for them, and re-layouts: 1.41 us -> none  [body(): return (gv, gg, gw, gt[:taps_n], gt[taps_n])]
    broadcast_in_dim x1 -> x0, local copies, waits for them, and re-layouts: 1.27 us -> none  [body(): gain[None, :]]
where the time goes in v2:
time: 70 us; the launch traced here: 69.1 us
  Pallas kernels  68.5 us (98%)
    pallas_call x1, Pallas kernels, body(): pl.pallas_call(functools.partial(kernel, (a, b, dp)), out_shape=(jax.Shap...  66.1 us
    pallas_call x1, Pallas kernels, body(): pl.pallas_call(finish, out_shape=(jax.ShapeDtypeStruct((tokens, width), B...  2.4 us

profile of v2, /device:TPU:0, one launch (start us, length us, event | category | flops | bytes accessed | tf_op | source)
XLA Modules:
  0.0 69.1 jit_solution(16628701602977685744)
XLA Ops:
  0.6 66.1 %shard_map.101 = (bf16[128,768]{1,0:T(8,128)(2,1)}, bf16[128,768]{1,0:T(8,128)(2,1)}, f32[256,768]{1,0:T(8,128)}, f32[32,768]{1,0:T(8,128)}) custom-call(bf16[128,768]{1,0:T(8,128)(2,1)} %val_in.1, bf16[128,768]{1,0:T(8,128)(2,1)} %gate_in.1, bf16[128,4096]{1,0:T(8,128)(2,1)} %cot.1, bf16[256,768]{1,0:T(8,128)(2,1)} %w.1, f32[31,768]{1,0:T(8,128)} %taps.1, ...), custom_call_target="tpu_custom_call" | custom-call | tf_op jit(solution)/shard_map/pallas_call | solution.py:432
  66.7 2.4 %shard_map.102 = (bf16[128,768]{1,0:T(8,128)(2,1)}, bf16[128,768]{1,0:T(8,128)(2,1)}, f32[256,768]{1,0:T(8,128)}, f32[31,768]{1,0:T(8,128)}, f32[768]{0:T(1024)}) custom-call(bf16[128,768]{1,0:T(8,128)(2,1)} %get-tuple-element.9.gv, bf16[128,768]{1,0:T(8,128)(2,1)} %get-tuple-element.10.gg, f32[256,768]{1,0:T(8,128)} %get-tuple-element.11.gw, ...), custom_call_target="tpu_custom_call" | custom-call | tf_op jit(solution)/shard_map/pallas_call | solution.py:446

commit v3 on v2

--- a/solution.py
+++ b/solution.py
@@ -170,12 +170,33 @@
         nrm[i] = normed
         dact[i] = sig * (1.0 + act * (1.0 - sig))
 
-    def sw_copy(h, j):
-        return remote(swg.at[h, own_rows, :], swg.at[h, own_rows, :],
-                      ss.at[h, j - 1], sr.at[h, j - 1], hi_peer(j))
-
-    for j in range(1, b):
-        sw_copy(0, j).start()
+    def sw_copy(step, up, source):
+        rows = swg.at[:, pl.ds(pl.multiple_of(source * tokens, tokens), tokens), :]
+        way = 0 if up else 1
+        return remote(rows, rows, ss.at[way, step], sr.at[way, step], hi_peer(1 if up else b - 1))
+
+    def sw_send(step, finish_it=False):
+        for up in (True, False):
+            source = hi - step if up else hi + step
+            here = (source >= 0) & (hi + 1 < b) if up else (source < b) & (hi > 0)
+
+            @pl.when(here)
+            def _():
+                copy = sw_copy(step, up, source)
+                if finish_it:
+                    copy.wait_send()
+                else:
+                    copy.start()
+
+    def sw_take(step):
+        for up in (True, False):
+            source = hi - 1 - step if up else hi + 1 + step
+
+            @pl.when(source >= 0 if up else source < b)
+            def _():
+                sw_copy(step, up, source).wait_recv()
+
+    sw_send(0)
 
     forwards = []
     for j in range(1, b):
@@ -195,7 +216,12 @@
     def mix_copy(h, j):
         return remote(mixs.at[h, j - 1], mixr.at[h, j - 1], ms.at[h, j - 1], mr.at[h, j - 1], hi_peer(j))
 
-    for h in range(parts):
+    step = 0
+    for h in range(parts):
+        if step < b - 2:
+            sw_take(step)
+            step += 1
+            sw_send(step)
         for copy in w_in[h]:
             copy.wait_recv()
 
@@ -206,10 +232,6 @@
             mixs[h, j - 1] = jnp.dot(block, wg[h], preferred_element_type=F32).astype(BF16)
             mix_copy(h, j).start()
 
-    for h in range(1, parts):
-        for j in range(1, b):
-            sw_copy(h, j).start()
-
     for h in range(parts):
         own_mix[h] = jnp.dot(cotg[own_rows, :], wg[h], preferred_element_type=F32)
     for q in range(a):
@@ -219,9 +241,6 @@
         return remote(gws.at[h, j - 1], gwr.at[h, j - 1], gs.at[h, j - 1], gr.at[h, j - 1], lo_peer(j))
 
     def gw_part(h):
-        for j in range(1, b):
-            sw_copy(h, j).wait_recv()
-
         @pl.loop(1, a)
         def _(j):
             other = lax.rem(lo + j, a)
@@ -231,7 +250,14 @@
 
         own_gw[h] = jnp.dot(cott[own_depth, :], swg[h], preferred_element_type=F32)
 
-    gw_part(0)
+    while step < b - 2:
+        sw_take(step)
+        step += 1
+        sw_send(step)
+    if b > 1:
+        sw_take(b - 2)
+    for h in range(parts):
+        gw_part(h)
 
     for h in range(parts):
         for j in range(1, b):
@@ -287,8 +313,6 @@
         copy.start()
         stage1.append(copy)
     sends += stage1
-    for h in range(1, parts - 1):
-        gw_part(h)
 
     halo2.wait_recv()
     keep_last = (s < sp - 1).astype(F32)
@@ -318,8 +342,6 @@
         copy.start()
         stage2.append(copy)
     sends += stage2
-    if parts > 1:
-        gw_part(parts - 1)
     for copy in stage2:
         copy.wait_recv()
     summed = r2[0]
@@ -348,9 +370,10 @@
 
     for copy in sends:
         copy.wait_send()
+    for step in range(b - 1):
+        sw_send(step, True)
     for h in range(parts):
         for j in range(1, b):
-            sw_copy(h, j).wait_send()
             mix_copy(h, j).wait_send()
         for j in range(1, a):
             gw_copy(h, j).wait_send()
@@ -420,7 +443,7 @@
         dma((b - 1, dp - 1)), dma((b - 1, dp - 1)),
         dma((parts, a - 1)), dma((parts, a - 1)),
         dma((dp - 1,)), dma((dp - 1,)), dma((dp - 1,)), dma((dp - 1,)),
-        dma((parts, b - 1)), dma((parts, b - 1)),
+        dma((2, b - 1)), dma((2, b - 1)),
         dma((parts, b - 1)), dma((parts, b - 1)),
         dma((parts, a - 1)), dma((parts, a - 1)),
         dma((a - 1,)), dma((a - 1,)),

time: 70 us -> 75.1 us (1.073)
  Pallas kernels: 68.5 us -> 72.9 us
    pallas_call x1, Pallas kernels: 66.1 us -> 70.5 us  [body(): pl.pallas_call(functools.partial(kernel, (a, b, dp)), out_shape=(jax.Shap...]
where the time goes in v3:
time: 75.1 us; the launch traced here: 73.6 us
  Pallas kernels  72.9 us (97%)
    pallas_call x1, Pallas kernels, body(): pl.pallas_call(functools.partial(kernel, (a, b, dp)), out_shape=(jax.Shap...  70.5 us
    pallas_call x1, Pallas kernels, body(): pl.pallas_call(finish, out_shape=(jax.ShapeDtypeStruct((tokens, width), B...  2.4 us

profile of v3, /device:TPU:0, one launch (start us, length us, event | category | flops | bytes accessed | tf_op | source)
XLA Modules:
  0.0 73.6 jit_solution(2060331372269591545)
XLA Ops:
  0.6 70.5 %shard_map.101 = (bf16[128,768]{1,0:T(8,128)(2,1)}, bf16[128,768]{1,0:T(8,128)(2,1)}, f32[256,768]{1,0:T(8,128)}, f32[32,768]{1,0:T(8,128)}) custom-call(bf16[128,768]{1,0:T(8,128)(2,1)} %val_in.1, bf16[128,768]{1,0:T(8,128)(2,1)} %gate_in.1, bf16[128,4096]{1,0:T(8,128)(2,1)} %cot.1, bf16[256,768]{1,0:T(8,128)(2,1)} %w.1, f32[31,768]{1,0:T(8,128)} %taps.1, ...), custom_call_target="tpu_custom_call" | custom-call | tf_op jit(solution)/shard_map/pallas_call | solution.py:455
  71.2 2.4 %shard_map.102 = (bf16[128,768]{1,0:T(8,128)(2,1)}, bf16[128,768]{1,0:T(8,128)(2,1)}, f32[256,768]{1,0:T(8,128)}, f32[31,768]{1,0:T(8,128)}, f32[768]{0:T(1024)}) custom-call(bf16[128,768]{1,0:T(8,128)(2,1)} %get-tuple-element.9.gv, bf16[128,768]{1,0:T(8,128)(2,1)} %get-tuple-element.10.gg, f32[256,768]{1,0:T(8,128)} %get-tuple-element.11.gw, ...), custom_call_target="tpu_custom_call" | custom-call | tf_op jit(solution)/shard_map/pallas_call | solution.py:469

commit v4 on v3

--- a/solution.py
+++ b/solution.py
@@ -216,12 +216,10 @@
     def mix_copy(h, j):
         return remote(mixs.at[h, j - 1], mixr.at[h, j - 1], ms.at[h, j - 1], mr.at[h, j - 1], hi_peer(j))
 
-    step = 0
-    for h in range(parts):
-        if step < b - 2:
-            sw_take(step)
-            step += 1
-            sw_send(step)
+    for step in range(b - 2):
+        sw_take(step)
+        sw_send(step + 1)
+    for h in range(parts):
         for copy in w_in[h]:
             copy.wait_recv()
 
@@ -250,13 +248,9 @@
 
         own_gw[h] = jnp.dot(cott[own_depth, :], swg[h], preferred_element_type=F32)
 
-    while step < b - 2:
-        sw_take(step)
-        step += 1
-        sw_send(step)
     if b > 1:
         sw_take(b - 2)
-    for h in range(parts):
+    for h in range(max(parts - 1, 1)):
         gw_part(h)
 
     for h in range(parts):
@@ -313,6 +307,8 @@
         copy.start()
         stage1.append(copy)
     sends += stage1
+    if parts > 1:
+        gw_part(parts - 1)
 
     halo2.wait_recv()
     keep_last = (s < sp - 1).astype(F32)

time: 75.1 us -> 67.1 us (0.89); the launches traced: 73.6 us -> 66.9 us
  Pallas kernels: 72.9 us -> 66.2 us
    pallas_call x1, Pallas kernels: 70.5 us -> 63.8 us  [body(): pl.pallas_call(functools.partial(kernel, (a, b, dp)), out_shape=(jax.Shap...]
where the time goes in v4:
time: 67.1 us; the launch traced here: 66.9 us
  Pallas kernels  66.2 us (99%)
    pallas_call x1, Pallas kernels, body(): pl.pallas_call(functools.partial(kernel, (a, b, dp)), out_shape=(jax.Shap...  63.8 us
    pallas_call x1, Pallas kernels, body(): pl.pallas_call(finish, out_shape=(jax.ShapeDtypeStruct((tokens, width), B...  2.4 us

profile of v4, /device:TPU:0, one launch (start us, length us, event | category | flops | bytes accessed | tf_op | source)
XLA Modules:
  0.0 66.9 jit_solution(1430444504306907337)
XLA Ops:
  0.6 63.8 %shard_map.101 = (bf16[128,768]{1,0:T(8,128)(2,1)}, bf16[128,768]{1,0:T(8,128)(2,1)}, f32[256,768]{1,0:T(8,128)}, f32[32,768]{1,0:T(8,128)}) custom-call(bf16[128,768]{1,0:T(8,128)(2,1)} %val_in.1, bf16[128,768]{1,0:T(8,128)(2,1)} %gate_in.1, bf16[128,4096]{1,0:T(8,128)(2,1)} %cot.1, bf16[256,768]{1,0:T(8,128)(2,1)} %w.1, f32[31,768]{1,0:T(8,128)} %taps.1, ...), custom_call_target="tpu_custom_call" | custom-call | tf_op jit(solution)/shard_map/pallas_call | solution.py:451
  64.5 2.4 %shard_map.102 = (bf16[128,768]{1,0:T(8,128)(2,1)}, bf16[128,768]{1,0:T(8,128)(2,1)}, f32[256,768]{1,0:T(8,128)}, f32[31,768]{1,0:T(8,128)}, f32[768]{0:T(1024)}) custom-call(bf16[128,768]{1,0:T(8,128)(2,1)} %get-tuple-element.9.gv, bf16[128,768]{1,0:T(8,128)(2,1)} %get-tuple-element.10.gg, f32[256,768]{1,0:T(8,128)} %get-tuple-element.11.gw, ...), custom_call_target="tpu_custom_call" | custom-call | tf_op jit(solution)/shard_map/pallas_call | solution.py:465

commit v5 on v4

--- a/solution.py
+++ b/solution.py
@@ -219,14 +219,20 @@
     for step in range(b - 2):
         sw_take(step)
         sw_send(step + 1)
-    for h in range(parts):
-        for copy in w_in[h]:
-            copy.wait_recv()
-
-        @pl.loop(1, b)
-        def _(j):
-            other = lax.rem(hi + j, b)
-            block = cotg[pl.ds(pl.multiple_of(other * tokens, tokens), tokens), :]
+    for copy in sum(w_in, []):
+        copy.wait_recv()
+    short = jnp.minimum(hi, b - 1 - hi)
+    longer = 1 - 2 * (hi > b - 1 - hi).astype(jnp.int32)
+
+    @pl.loop(0, b - 1)
+    def _(o):
+        near = (o // 2 + 1) * (1 - 2 * lax.rem(o, 2))
+        far = longer * (o - short + 1)
+        move = jnp.where(o < 2 * short, near, far)
+        j = lax.rem(move + b, b)
+        other = hi + move
+        block = cotg[pl.ds(pl.multiple_of(other * tokens, tokens), tokens), :]
+        for h in range(parts):
             mixs[h, j - 1] = jnp.dot(block, wg[h], preferred_element_type=F32).astype(BF16)
             mix_copy(h, j).start()
 

time: 67.1 us -> 66.6 us (level)
  no operation moved by 1% of the time
where the time goes in v5:
time: 66.6 us; the launch traced here: 66.4 us
  Pallas kernels  65.7 us (99%)
    pallas_call x1, Pallas kernels, body(): pl.pallas_call(functools.partial(kernel, (a, b, dp)), out_shape=(jax.Shap...  63.3 us
    pallas_call x1, Pallas kernels, body(): pl.pallas_call(finish, out_shape=(jax.ShapeDtypeStruct((tokens, width), B...  2.4 us

profile of v5, /device:TPU:0, one launch (start us, length us, event | category | flops | bytes accessed | tf_op | source)
XLA Modules:
  0.0 66.4 jit_solution(14546406534785820491)
XLA Ops:
  0.6 63.3 %shard_map.101 = (bf16[128,768]{1,0:T(8,128)(2,1)}, bf16[128,768]{1,0:T(8,128)(2,1)}, f32[256,768]{1,0:T(8,128)}, f32[32,768]{1,0:T(8,128)}) custom-call(bf16[128,768]{1,0:T(8,128)(2,1)} %val_in.1, bf16[128,768]{1,0:T(8,128)(2,1)} %gate_in.1, bf16[128,4096]{1,0:T(8,128)(2,1)} %cot.1, bf16[256,768]{1,0:T(8,128)(2,1)} %w.1, f32[31,768]{1,0:T(8,128)} %taps.1, ...), custom_call_target="tpu_custom_call" | custom-call | tf_op jit(solution)/shard_map/pallas_call | solution.py:457
  64.0 2.4 %shard_map.102 = (bf16[128,768]{1,0:T(8,128)(2,1)}, bf16[128,768]{1,0:T(8,128)(2,1)}, f32[256,768]{1,0:T(8,128)}, f32[31,768]{1,0:T(8,128)}, f32[768]{0:T(1024)}) custom-call(bf16[128,768]{1,0:T(8,128)(2,1)} %get-tuple-element.9.gv, bf16[128,768]{1,0:T(8,128)(2,1)} %get-tuple-element.10.gg, f32[256,768]{1,0:T(8,128)} %get-tuple-element.11.gw, ...), custom_call_target="tpu_custom_call" | custom-call | tf_op jit(solution)/shard_map/pallas_call | solution.py:471
